TPU v7x, 32 devices: a whole 2x2x4 slice. The times are simulated.
32 devices in a mesh: rep: 2 (over x), fs: 8 (over z, y), tp: 2 (over core).
Axes of the slice: x: 2, y: 2, z: 4, core: 2. Of those that a mesh axis runs over, the one named last changes fastest.
Arguments:
- tokens: bfloat16 [16384, 2048], P(('rep', 'fs'), 'tp'), may hold values from -6 to 6
- attention_pre_gain: float32 [2048], replicated, may hold values from 0.1 to 1.9
- query_matrix: bfloat16 [2048, 512], P('fs', 'tp'), may hold values from -0.125 to 0.125
- key_matrix: bfloat16 [2048, 512], P('fs', 'tp'), may hold values from -0.125 to 0.125
- value_matrix: bfloat16 [2048, 1024], P('fs', 'tp'), may hold values from -0.125 to 0.125
- decay_first_weight: bfloat16 [2048, 16], replicated, may hold values from -0.125 to 0.125
- decay_second_weight: bfloat16 [16, 512], P(None, 'tp'), may hold values from -1.5 to 1.5
- decay_offset_bias: float32 [512], P('tp'), may hold values from 0 to 6
- extra_log_surge: float32 [16384, 2], P(('rep', 'fs'), 'tp'), may hold values from -0.7 to 0
- readout_head_gain: float32 [512], replicated, may hold values from 0.1 to 1.9
- output_matrix: bfloat16 [1024, 2048], P('tp', 'fs'), may hold values from -2.4375 to 2.4375
- attention_post_gain: float32 [2048], P('tp'), may hold values from 0.1 to 1.9
- feedforward_pre_gain: float32 [2048], replicated, may hold values from 0.1 to 1.9
- up_matrix: bfloat16 [2048, 4096], P('fs', 'tp'), may hold values from -0.125 to 0.125
- down_matrix: bfloat16 [4096, 2048], P('tp', 'fs'), may hold values from -1.21875 to 1.21875
- feedforward_post_gain: float32 [2048], P('tp'), may hold values from 0.1 to 1.9
Outputs:
- layer_out: bfloat16 [16384, 2048], P(('rep', 'fs'), 'tp')
All inputs are finite; a program needn't handle non-finite values.
Results may differ from a plain program's by a relative error of at most 0.017.
Values may be sent and summed in bfloat16 or wider, within the bound.
A program may use at most 128 MiB of HBM per device.

v0:
```python
import jax
import jax.numpy as jnp
from jax import lax
from jax.sharding import PartitionSpec as P

KEY_WIDTH = 256
DV = 512
BLOCK = 64
EPS = 1e-06


def pre_norm(rows, gain):
    values = rows.astype(jnp.float32)
    scale = lax.rsqrt(jnp.mean(values * values, axis=-1, keepdims=True) + EPS)
    return (values * scale * gain).astype(jnp.bfloat16)


def block_attention(queries, keys_in, values_in, log_gates):
    head_count, token_length, key_size = queries.shape
    value_size = values_in.shape[-1]
    blocks = token_length // BLOCK

    def to_blocks(array):
        return array.reshape(head_count, blocks, BLOCK, array.shape[-1]).transpose(1, 0, 2, 3)

    causal = jnp.tril(jnp.ones((BLOCK, BLOCK), dtype=bool))[None, :, :, None]
    highest = lax.Precision.HIGHEST

    def advance(memory_state, inputs):
        query_blk, key_blk, value_blk, gate_blk = inputs
        cumulative = jnp.cumsum(gate_blk, axis=1)
        carried = jnp.einsum(
            "hid,hde->hie", query_blk * jnp.exp(cumulative), memory_state, precision=highest
        )
        spread_log = cumulative[:, :, None, :] - cumulative[:, None, :, :]
        weights = jnp.exp(jnp.where(causal, spread_log, -jnp.inf))
        scores = jnp.einsum("hid,hjd,hijd->hij", query_blk, key_blk, weights, precision=highest)
        readout = carried + jnp.einsum("hij,hje->hie", scores, value_blk, precision=highest)
        final_log = cumulative[:, -1:, :]
        memory_state = jnp.exp(final_log[:, 0, :])[:, :, None] * memory_state + jnp.einsum(
            "hjd,hje->hde", key_blk * jnp.exp(final_log - cumulative), value_blk, precision=highest
        )
        return (memory_state, readout)

    start_state = jnp.zeros((head_count, key_size, value_size), jnp.float32)
    _, readout = lax.scan(
        advance,
        start_state,
        (to_blocks(queries), to_blocks(keys_in), to_blocks(values_in), to_blocks(log_gates)),
    )
    return readout.transpose(1, 0, 2, 3).reshape(head_count, token_length, value_size)


def make_adder(left):

    def add_rows(total, piece, start):
        return jnp.dot(left, piece, preferred_element_type=jnp.float32)

    return add_rows


def make_projector(left, piece):
    return jnp.dot(left, piece, preferred_element_type=jnp.float32)


def on_device(
    tokens,
    attention_pre_gain,
    query_matrix,
    key_matrix,
    value_matrix,
    decay_first_weight,
    decay_second_weight,
    decay_offset_bias,
    extra_log_surge,
    readout_head_gain,
    output_matrix,
    attention_post_gain,
    feedforward_pre_gain,
    up_matrix,
    down_matrix,
    feedforward_post_gain,
):
    token_length = tokens.shape[0]
    gathered = lax.all_gather(tokens, "tp", axis=1, tiled=True)
    width = gathered.shape[1]
    normed = pre_norm(gathered, attention_pre_gain)
    add_rows = make_adder(normed)
    key_cols = query_matrix.shape[1]
    value_cols = value_matrix.shape[1]
    empty_key = jnp.zeros((token_length, key_cols), jnp.float32)
    empty_value = jnp.zeros((token_length, value_cols), jnp.float32)
    start = jnp.int32(0)
    query_proj = add_rows(empty_key, lax.all_gather(query_matrix, "fs", axis=0, tiled=True), start)
    key_proj = add_rows(empty_key, lax.all_gather(key_matrix, "fs", axis=0, tiled=True), start)
    value_proj = add_rows(
        empty_value, lax.all_gather(value_matrix, "fs", axis=0, tiled=True), start
    )
    query_proj = query_proj.astype(jnp.bfloat16)
    key_proj = key_proj.astype(jnp.bfloat16)
    value_proj = value_proj.astype(jnp.bfloat16)
    rank_rows = jnp.dot(normed, decay_first_weight, preferred_element_type=jnp.float32).astype(
        jnp.bfloat16
    )
    gate_source_input = (
        jnp.dot(rank_rows, decay_second_weight, preferred_element_type=jnp.float32)
        + decay_offset_bias
    )
    head_count = key_cols // KEY_WIDTH
    logarithm_decay = (jax.nn.log_sigmoid(gate_source_input) / 16.0).reshape(
        token_length, head_count, KEY_WIDTH
    ) + extra_log_surge[:, :, None]

    def by_head(array, size):
        return array.astype(jnp.float32).reshape(token_length, head_count, size).transpose(1, 0, 2)

    queries = by_head(query_proj, KEY_WIDTH) * KEY_WIDTH ** (-0.5)
    readout = block_attention(
        queries,
        by_head(key_proj, KEY_WIDTH),
        by_head(value_proj, DV),
        logarithm_decay.transpose(1, 0, 2),
    )
    readout = readout.transpose(1, 0, 2)
    head_scale = lax.rsqrt(jnp.mean(readout * readout, axis=-1, keepdims=True) + EPS)
    mixed = (
        (readout * head_scale * readout_head_gain)
        .astype(jnp.bfloat16)
        .reshape(token_length, value_cols)
    )
    partial_attn = make_projector(mixed, lax.all_gather(output_matrix, "fs", axis=1, tiled=True))
    attn = lax.psum_scatter(
        partial_attn.astype(jnp.bfloat16), "tp", scatter_dimension=1, tiled=True
    ).astype(jnp.float32)
    attn_total = lax.psum(jnp.sum(attn * attn, axis=1), "tp")
    attn_scale = lax.rsqrt(attn_total / width + EPS)[:, None]
    resid = (tokens.astype(jnp.float32) + attn * attn_scale * attention_post_gain).astype(
        jnp.bfloat16
    )
    gathered_mid = lax.all_gather(resid, "tp", axis=1, tiled=True)
    normed_mid = pre_norm(gathered_mid, feedforward_pre_gain)
    whole_up = lax.all_gather(up_matrix, "fs", axis=0, tiled=True)
    hidden = jnp.dot(normed_mid, whole_up, preferred_element_type=jnp.float32)
    hidden = jax.nn.relu(hidden)
    squared = (hidden * hidden).astype(jnp.bfloat16)
    partial_feed = make_projector(squared, lax.all_gather(down_matrix, "fs", axis=1, tiled=True))
    feed = lax.psum_scatter(
        partial_feed.astype(jnp.bfloat16), "tp", scatter_dimension=1, tiled=True
    ).astype(jnp.float32)
    feed_total = lax.psum(jnp.sum(feed * feed, axis=1), "tp")
    feed_scale = lax.rsqrt(feed_total / width + EPS)[:, None]
    return (resid.astype(jnp.float32) + feed * feed_scale * feedforward_post_gain).astype(
        jnp.bfloat16
    )


def solution(mesh):
    return jax.shard_map(
        on_device,
        mesh=mesh,
        in_specs=(
            P(("rep", "fs"), "tp"),
            P(),
            P("fs", "tp"),
            P("fs", "tp"),
            P("fs", "tp"),
            P(),
            P(None, "tp"),
            P("tp"),
            P(("rep", "fs"), "tp"),
            P(),
            P("tp", "fs"),
            P("tp"),
            P(),
            P("fs", "tp"),
            P("tp", "fs"),
            P("tp"),
        ),
        out_specs=P(("rep", "fs"), "tp"),
        check_vma=False,
    )
```

profile of v0, /device:TPU:0, one launch (start us, length us, event | category | flops | bytes accessed | tf_op | source)
XLA Modules:
  0.0 660.1 jit_solution(7252431059757820232)
XLA Ops:
  10.0 15.3 %all-gather.9.cloned.1.call-done = bf16[1024,2048]{1,0:T(8,128)(2,1)} async-done(((bf16[1024,1024]{1,0:T(8,128)(2,1)}), bf16[1024,2048]{1,0:T(8,128)(2,1)}) %all-gather.9.cloned.1.call-update) | async-done | bytes 4194320 | tf_op jit(solution)/shard_map/all_gather | solution.py:85
  25.3 3.2 fusion.30
  28.8 3.0 fusion.32
  31.7 46.0 %all-gather.13.cloned.1.call-done = bf16[2048,512]{1,0:T(8,128)(2,1)} async-done(((bf16[256,512]{1,0:T(8,128)(2,1)}), bf16[2048,512]{1,0:T(8,128)(2,1)}) %all-gather.13.cloned.1.call-update) | async-done | bytes 2097168 | tf_op jit(solution)/shard_map/all_gather | solution.py:97
  77.7 5.2 convolution_convert_fusion.1
  84.5 34.2 %all-gather.11.cloned.1.call-done = bf16[2048,256]{1,0:T(8,128)(2,1)} async-done(((bf16[256,256]{1,0:T(8,128)(2,1)}), bf16[2048,256]{1,0:T(8,128)(2,1)}) %all-gather.11.cloned.1.call-update) | async-done | bytes 1048592 | tf_op jit(solution)/shard_map/all_gather | solution.py:95
  118.7 3.7 convolution_convert_fusion.3
  123.6 5.1 fusion.63
  128.7 31.0 %all-gather.15.cloned.1.call-done = bf16[2048,256]{1,0:T(8,128)(2,1)} async-done(((bf16[256,256]{1,0:T(8,128)(2,1)}), bf16[2048,256]{1,0:T(8,128)(2,1)}) %all-gather.15.cloned.1.call-update) | async-done | bytes 1048592 | tf_op jit(solution)/shard_map/all_gather | solution.py:94
  159.7 4.8 fusion.60
  164.5 150.9 %while.13 = (s32[]{:T(128)}, f32[1,256,512]{2,1,0:T(8,128)S(1)}, f32[16,1,64,512]{3,2,1,0:T(8,128)S(1)}, f32[16,1,64,256]{3,2,1,0:T(8,128)}, f32[16,1,64,256]{3,...) while((s32[]{:T(128)}, f32[1,256,512]{2,1,0:T(8,128)S(1)}, ...), condition=%wide.region_3.4_spmd.clone, body=%wide.region_1.3_spmd.clone.sunk | while | flops 233373696 | bytes 11649660 | solution.py:46
  167.2 2.5 fusion.98
  172.3 1.6 fusion.96
  176.6 2.5 fusion.98
  186.1 2.5 fusion.98
  191.1 1.6 fusion.96
  195.5 2.5 fusion.98
  200.6 1.6 fusion.96
  204.9 2.5 fusion.98
  214.4 2.5 fusion.98
  219.4 1.6 fusion.96
  223.8 2.5 fusion.98
  228.9 1.6 fusion.96
  233.2 2.5 fusion.98
  238.3 1.6 fusion.96
  242.7 2.5 fusion.98
  247.7 1.6 fusion.96
  252.1 2.5 fusion.98
  261.5 2.5 fusion.98
  270.9 2.5 fusion.98
  280.4 2.5 fusion.98
  289.8 2.5 fusion.98
  299.2 2.5 fusion.98
  308.7 2.5 fusion.98
  316.0 5.9 convolution_convert_fusion
  322.0 10.7 %reduce-scatter.3.cloned.1.call-done = bf16[1024,1024]{1,0:T(8,128)(2,1)} async-done(((bf16[1024,2048]{1,0:T(8,128)(2,1)}), bf16[1024,1024]{1,0:T(8,128)(2,1)}) %reduce-scatter.3.cloned.1.call-update) | async-done | bytes 2097168 | tf_op jit(solution)/shard_map/reduce_scatter | solution.py:132
  332.6 2.1 fusion.36
  334.7 2.5 psum.14
  337.2 3.7 fusion.39
  342.5 13.6 %all-gather.19.cloned.1.call-done = bf16[1024,2048]{1,0:T(8,128)(2,1)} async-done(((bf16[1024,1024]{1,0:T(8,128)(2,1)}), bf16[1024,2048]{1,0:T(8,128)(2,1)}) %all-gather.19.cloned.1.call-update) | async-done | bytes 4194320 | tf_op jit(solution)/shard_map/all_gather | solution.py:140
  356.1 3.1 fusion.33
  359.2 124.7 %all-gather.21.cloned.1.call-done = bf16[2048,2048]{1,0:T(8,128)(2,1)} async-done(((bf16[256,2048]{1,0:T(8,128)(2,1)}), bf16[2048,2048]{1,0:T(8,128)(2,1)}) %all-gather.21.cloned.1.call-update) | async-done | bytes 8388624 | tf_op jit(solution)/shard_map/all_gather | solution.py:142
  483.9 125.2 %all-gather.23.cloned.1.call-done = bf16[2048,2048]{1,0:T(8,128)(2,1)} async-done(((bf16[2048,256]{1,0:T(8,128)(2,1)}), bf16[2048,2048]{1,0:T(8,128)(2,1)}) %all-gather.23.cloned.1.call-update) | async-done | bytes 8388624 | tf_op jit(solution)/shard_map/all_gather | solution.py:146
  609.1 25.6 %fusion.53 = bf16[1024,2048]{1,0:T(8,128)(2,1)} fusion(bf16[2048,2048]{1,0:T(8,128)(2,1)} %all-gather.23.cloned.1.call-done, bf16[2048,2048]{1,0:T(8,128)(2,1)} %all-gather.21.cloned.1.call-done, bf16[1024,2048]{1,0:T(8,128)(2,1)} %all-gather.19.cloned.1.call-done, f32[2048]{0:T(1024)S(1)} %copy-done.10, f32[1024]{0:T(1024)S(1)} %add_rsqrt_fusion.2), kind=kOutput, calls=%fused_computation.65 | convolution fusion | flops 17196646400 | bytes 25178112 | tf_op jit(solution)/shard_map/dot_general | solution.py:63
  634.7 10.2 %reduce-scatter.5.cloned.1.call-done = bf16[1024,1024]{1,0:T(8,128)(2,1)} async-done(((bf16[1024,2048]{1,0:T(8,128)(2,1)}), bf16[1024,1024]{1,0:T(8,128)(2,1)}) %reduce-scatter.5.cloned.1.call-update) | async-done | bytes 2097168 | tf_op jit(solution)/shard_map/reduce_scatter | solution.py:147
  644.9 2.1 fusion.40
  647.0 2.5 psum.15
  649.5 3.7 fusion.43
  (212 shorter events, 106.7 us)
Async XLA Ops:
  6.5 117.0 %copy-start = (bf16[2048,16]{0,1:T(8,128)(2,1)S(1)}, bf16[2048,16]{0,1:T(8,128)(2,1)}, u32[]{:S(2)}) copy-start(bf16[2048,16]{0,1:T(8,128)(2,1)} %param.23) | copy-start | bytes 196612
  6.5 22.0 %copy-start.5 = (f32[2048]{0:T(1024)S(1)}, f32[2048]{0:T(1024)}, u32[]{:S(2)}) copy-start(f32[2048]{0:T(1024)} %param.19) | copy-start | bytes 24580
  6.5 18.8 %all-gather.9.cloned.1.call-start = ((), (), s32[]{:S(2)}) async-start(), calls=%async_computation.2 | async-start | bytes 6291456 | tf_op jit(solution)/shard_map/all_gather | solution.py:85
  7.3 70.5 %all-gather.13.cloned.1.call-start = ((), (), s32[]{:S(2)}) async-start(), calls=%async_computation.4 | async-start | bytes 2359296 | tf_op jit(solution)/shard_map/all_gather | solution.py:97
  8.0 110.7 %all-gather.11.cloned.1.call-start = ((), (), s32[]{:S(2)}) async-start(), calls=%async_computation.3 | async-start | bytes 1179648 | tf_op jit(solution)/shard_map/all_gather | solution.py:95
  8.7 151.0 %all-gather.15.cloned.1.call-start = ((), (), s32[]{:S(2)}) async-start(), calls=%async_computation.5 | async-start | bytes 1179648 | tf_op jit(solution)/shard_map/all_gather | solution.py:94
  9.3 306.7 %all-gather.17.cloned.1.call-start = ((), (), s32[]{:S(2)}) async-start(), calls=%async_computation.6 | async-start | bytes 2359296 | tf_op jit(solution)/shard_map/all_gather | solution.py:131
  9.9 322.7 %reduce-scatter.3.cloned.1.call-start = ((), (), s32[]{:S(2)}) async-start(), calls=%async_computation.7 | async-start | bytes 6291456 | tf_op jit(solution)/shard_map/reduce_scatter | solution.py:132
  25.3 3.4 copy-start.3
  84.5 39.0 %copy-start.9 = (bf16[16,256]{1,0:T(8,128)(2,1)S(1)}, bf16[16,256]{1,0:T(8,128)(2,1)}, u32[]{:S(2)}) copy-start(bf16[16,256]{1,0:T(8,128)(2,1)} %param.24) | copy-start | bytes 24580
  84.5 39.0 %copy-start.11 = (f32[1024,1]{0,1:T(1,128)S(1)}, f32[1024,1]{0,1:T(1,128)}, u32[]{:S(2)}) copy-start(f32[1024,1]{0,1:T(1,128)} %param.26) | copy-start | bytes 12292
  84.5 39.0 %copy-start.12 = (f32[256]{0:T(256)S(1)}, f32[256]{0:T(256)}, u32[]{:S(2)}) copy-start(f32[256]{0:T(256)} %param.25) | copy-start | bytes 3076
  164.5 151.2 %copy-start.8 = (f32[512]{0:T(512)S(1)}, f32[512]{0:T(512)}, u32[]{:S(2)}) copy-start(f32[512]{0:T(512)} %param.27) | copy-start | bytes 6148
  321.9 15.3 %copy-start.4 = (bf16[1024,1024]{1,0:T(8,128)(2,1)S(1)}, bf16[1024,1024]{1,0:T(8,128)(2,1)}, u32[]{:S(2)}) copy-start(bf16[1024,1024]{1,0:T(8,128)(2,1)} %param.18) | copy-start | bytes 6291460
  321.9 15.3 %copy-start.6 = (f32[1024]{0:T(1024)S(1)}, f32[1024]{0:T(1024)}, u32[]{:S(2)}) copy-start(f32[1024]{0:T(1024)} %param.29) | copy-start | bytes 12292
  321.9 34.2 %all-gather.19.cloned.1.call-start = ((), (), s32[]{:S(2)}) async-start(), calls=%async_computation.8 | async-start | bytes 6291456 | tf_op jit(solution)/shard_map/all_gather | solution.py:140
  340.9 268.2 %copy-start.10 = (f32[2048]{0:T(1024)S(1)}, f32[2048]{0:T(1024)}, u32[]{:S(2)}) copy-start(f32[2048]{0:T(1024)} %param.30) | copy-start | bytes 24580
  341.0 142.9 %all-gather.21.cloned.1.call-start = ((), (), s32[]{:S(2)}) async-start(), calls=%async_computation.9 | async-start | bytes 9437184 | tf_op jit(solution)/shard_map/all_gather | solution.py:142
  341.7 267.4 %all-gather.23.cloned.1.call-start = ((), (), s32[]{:S(2)}) async-start(), calls=%async_computation.10 | async-start | bytes 9437184 | tf_op jit(solution)/shard_map/all_gather | solution.py:146
  342.4 302.5 %reduce-scatter.5.cloned.1.call-start = ((), (), s32[]{:S(2)}) async-start(), calls=%async_computation.11 | async-start | bytes 6291456 | tf_op jit(solution)/shard_map/reduce_scatter | solution.py:147
  634.7 14.8 %copy-start.2 = (bf16[1024,1024]{1,0:T(8,128)(2,1)S(1)}, bf16[1024,1024]{1,0:T(8,128)(2,1)}, u32[]{:S(2)}) copy-start(bf16[1024,1024]{1,0:T(8,128)(2,1)} %fusion.39) | copy-start | bytes 6291460
  634.7 14.8 %copy-start.7 = (f32[1024]{0:T(1024)S(1)}, f32[1024]{0:T(1024)}, u32[]{:S(2)}) copy-start(f32[1024]{0:T(1024)} %param.33) | copy-start | bytes 12292
  634.7 18.5 %copy-start.1 = (bf16[2048,16]{0,1:T(8,128)(2,1)S(1)}, bf16[2048,16]{0,1:T(8,128)(2,1)}, u32[]{:S(2)}) copy-start(bf16[2048,16]{0,1:T(8,128)(2,1)} %param.23) | copy-start | bytes 196612
Sparse Core Ops, SparseCore 0:
  8.9 16.3 all-gather.8
  27.4 50.2 all-gather.12
  79.8 38.7 all-gather.10
  120.7 38.9 all-gather.14
  161.6 49.1 all-gather.16
  322.0 10.5 reduce-scatter.2
  341.1 14.9 all-gather.18
  358.2 125.6 all-gather.20
  485.9 123.1 all-gather.22
  634.9 10.0 reduce-scatter.4
where the time goes:
time: 663 us; the launch traced here: 660 us
  waiting for transfers between devices  415 us (63%)
  matrix products  117 us (18%)
  other arithmetic  79.4 us (12%)
  local copies, waits for them, and re-layouts  28.2 us (4%)
  between operations  13.7 us (2%)
    all_gather x1, waiting for transfers between devices, on_device(): lax.all_gather(down_matrix, 'fs', axis=1, tiled=True)  125 us
    all_gather x1, waiting for transfers between devices, on_device(): whole_up = lax.all_gather(up_matrix, 'fs', axis=0, tiled=True)  125 us
    all_gather x1, waiting for transfers between devices, on_device(): lax.all_gather(value_matrix, 'fs', axis=0, tiled=True)  46 us
    dot_general x16, other arithmetic, advance(): jnp.einsum('hid,hjd,hijd->hij', query_blk, key_blk, weights, precision=hi...  40.2 us
    all_gather x1, waiting for transfers between devices, on_device(): lax.all_gather(key_matrix, 'fs', axis=0, tiled=True)  34.2 us
    dot_general x2, matrix products, make_projector(): return jnp.dot(left, piece, preferred_element_type=jnp.float32)  31.5 us
    all_gather x1, waiting for transfers between devices, on_device(): lax.all_gather(query_matrix, 'fs', axis=0, tiled=True)  31 us
    dot_general x16, matrix products, advance(): jnp.einsum('hjd,hje->hde', key_blk * jnp.exp(final_log - cumulative), val...  26.3 us
  transfers between devices with their start and end apart: 10, of which 9 were waited for; matrix products, arithmetic and copies ran while one was open for 27% of the time, Pallas kernels for 0%

commit v1 on v0

--- a/solution.py
+++ b/solution.py
@@ -139,7 +139,12 @@
     )
     gathered_mid = lax.all_gather(resid, "tp", axis=1, tiled=True)
     normed_mid = pre_norm(gathered_mid, feedforward_pre_gain)
-    whole_up = lax.all_gather(up_matrix, "fs", axis=0, tiled=True)
+    ring = [up_matrix]
+    for hop in range(7):
+        ring.append(lax.ppermute(ring[-1], "fs", [(dev, (dev + 1) % 8) for dev in range(8)]))
+    whole_up = jnp.roll(
+        jnp.concatenate(ring[::-1], axis=0), (lax.axis_index("fs") + 1) * ring[0].shape[0], axis=0
+    )
     hidden = jnp.dot(normed_mid, whole_up, preferred_element_type=jnp.float32)
     hidden = jax.nn.relu(hidden)
     squared = (hidden * hidden).astype(jnp.bfloat16)

time: 663 us -> 695 us (1.048)
  local copies, waits for them, and re-layouts: 28.2 us -> 53.3 us
    ppermute x0 -> x7, waiting for transfers between devices: none -> 267 us  [on_device(): lax.ppermute(ring[-1], 'fs', [(dev, (dev + 1) % 8) for dev in range(8)])]
    all_gather x1, waiting for transfers between devices: 125 us -> 0.02 us  [on_device(): lax.all_gather(down_matrix, 'fs', axis=1, tiled=True)]
    all_gather x1 -> x0, waiting for transfers between devices: 125 us -> none  [on_device(): whole_up = lax.all_gather(up_matrix, 'fs', axis=0, tiled=True)]
    unnamed x26 -> x55, local copies, waits for them, and re-layouts: 0.25 us -> 24.3 us
    all_gather x1, waiting for transfers between devices: 13.6 us -> 0.01 us  [on_device(): gathered_mid = lax.all_gather(resid, 'tp', axis=1, tiled=True)]
  transfers between devices with their start and end apart: 10 -> 16, of which waited for: 9 -> 13; matrix products, arithmetic and copies ran while one was open for 27% -> 29% of each run, Pallas kernels for 0% -> 0%
where the time goes in v1:
time: 695 us; the launch traced here: 692 us
  waiting for transfers between devices  420 us (60%)
  matrix products  117 us (17%)
  other arithmetic  79.5 us (11%)
  local copies, waits for them, and re-layouts  53.3 us (8%)
  between operations  13.4 us (2%)
    ppermute x7, waiting for transfers between devices, on_device(): lax.ppermute(ring[-1], 'fs', [(dev, (dev + 1) % 8) for dev in range(8)])  267 us
    all_gather x1, waiting for transfers between devices, on_device(): lax.all_gather(value_matrix, 'fs', axis=0, tiled=True)  46 us
    dot_general x16, other arithmetic, advance(): jnp.einsum('hid,hjd,hijd->hij', query_blk, key_blk, weights, precision=hi...  40.2 us
    all_gather x1, waiting for transfers between devices, on_device(): lax.all_gather(key_matrix, 'fs', axis=0, tiled=True)  34.2 us
    dot_general x2, matrix products, make_projector(): return jnp.dot(left, piece, preferred_element_type=jnp.float32)  31.7 us
    all_gather x1, waiting for transfers between devices, on_device(): lax.all_gather(query_matrix, 'fs', axis=0, tiled=True)  31 us
    dot_general x16, matrix products, advance(): jnp.einsum('hjd,hje->hde', key_blk * jnp.exp(final_log - cumulative), val...  26.3 us
    unnamed x55, local copies, waits for them, and re-layouts  24.3 us
  transfers between devices with their start and end apart: 16, of which 13 were waited for; matrix products, arithmetic and copies ran while one was open for 29% of the time, Pallas kernels for 0%

profile of v1, /device:TPU:0, one launch (start us, length us, event | category | flops | bytes accessed | tf_op | source)
XLA Modules:
  0.0 691.7 jit_solution(15321990995125744202)
XLA Ops:
  10.0 15.3 %all-gather.8.cloned.1.call-done = bf16[1024,2048]{1,0:T(8,128)(2,1)} async-done(((bf16[1024,1024]{1,0:T(8,128)(2,1)}), bf16[1024,2048]{1,0:T(8,128)(2,1)}) %all-gather.8.cloned.1.call-update) | async-done | bytes 4194320 | tf_op jit(solution)/shard_map/all_gather | solution.py:85
  25.3 3.2 fusion.30
  28.8 3.0 fusion.32
  31.7 46.0 %all-gather.12.cloned.1.call-done = bf16[2048,512]{1,0:T(8,128)(2,1)} async-done(((bf16[256,512]{1,0:T(8,128)(2,1)}), bf16[2048,512]{1,0:T(8,128)(2,1)}) %all-gather.12.cloned.1.call-update) | async-done | bytes 2097168 | tf_op jit(solution)/shard_map/all_gather | solution.py:97
  77.7 5.2 convolution_convert_fusion.1
  84.5 34.2 %all-gather.10.cloned.1.call-done = bf16[2048,256]{1,0:T(8,128)(2,1)} async-done(((bf16[256,256]{1,0:T(8,128)(2,1)}), bf16[2048,256]{1,0:T(8,128)(2,1)}) %all-gather.10.cloned.1.call-update) | async-done | bytes 1048592 | tf_op jit(solution)/shard_map/all_gather | solution.py:95
  118.7 3.7 convolution_convert_fusion.3
  123.6 5.1 fusion.70
  128.7 31.0 %all-gather.14.cloned.1.call-done = bf16[2048,256]{1,0:T(8,128)(2,1)} async-done(((bf16[256,256]{1,0:T(8,128)(2,1)}), bf16[2048,256]{1,0:T(8,128)(2,1)}) %all-gather.14.cloned.1.call-update) | async-done | bytes 1048592 | tf_op jit(solution)/shard_map/all_gather | solution.py:94
  159.7 4.8 fusion.67
  164.5 150.9 %while.13 = (s32[]{:T(128)}, f32[1,256,512]{2,1,0:T(8,128)S(1)}, f32[16,1,64,512]{3,2,1,0:T(8,128)S(1)}, f32[16,1,64,256]{3,2,1,0:T(8,128)}, f32[16,1,64,256]{3,...) while((s32[]{:T(128)}, f32[1,256,512]{2,1,0:T(8,128)S(1)}, ...), condition=%wide.region_3.4_spmd.clone, body=%wide.region_1.3_spmd.clone.sunk | while | flops 233373696 | bytes 11649660 | solution.py:46
  167.2 2.5 fusion.106
  176.6 2.5 fusion.106
  186.1 2.5 fusion.106
  195.5 2.5 fusion.106
  204.9 2.5 fusion.106
  214.4 2.5 fusion.106
  223.8 2.5 fusion.106
  233.2 2.5 fusion.106
  242.7 2.5 fusion.106
  252.1 2.5 fusion.106
  261.5 2.5 fusion.106
  270.9 2.5 fusion.106
  280.4 2.5 fusion.106
  289.8 2.5 fusion.106
  299.2 2.5 fusion.106
  308.7 2.5 fusion.106
  316.0 5.9 convolution_convert_fusion
  321.9 10.7 %reduce-scatter.3.cloned.1.call-done = bf16[1024,1024]{1,0:T(8,128)(2,1)} async-done(((bf16[1024,2048]{1,0:T(8,128)(2,1)}), bf16[1024,1024]{1,0:T(8,128)(2,1)}) %reduce-scatter.3.cloned.1.call-update) | async-done | bytes 2097168 | tf_op jit(solution)/shard_map/reduce_scatter | solution.py:132
  332.6 2.1 fusion.38
  334.7 2.5 psum.14
  337.2 3.8 fusion.41
  343.7 26.3 %collective-permute-done = bf16[256,2048]{1,0:T(8,128)(2,1)S(1)} collective-permute-done((bf16[256,2048]{1,0:T(8,128)(2,1)S(1)}, bf16[256,2048]{1,0:T(8,128)(2,1)S(1)}, u32[]{:S(2)}, u32[]{:S(2)}) %collective-permute-start) | collective-permute-done | bytes 1048608 | tf_op jit(solution)/shard_map/ppermute | solution.py:144
  370.0 48.4 %collective-permute-done.1 = bf16[256,2048]{1,0:T(8,128)(2,1)S(1)} collective-permute-done((bf16[256,2048]{1,0:T(8,128)(2,1)S(1)}, bf16[256,2048]{1,0:T(8,128)(2,1)S(1)}, u32[]{:S(2)}, u32[]{:S(2)}) %collective-permute-start.1) | collective-permute-done | bytes 1048608 | tf_op jit(solution)/shard_map/ppermute | solution.py:144
  418.4 42.5 %collective-permute-done.2 = bf16[256,2048]{1,0:T(8,128)(2,1)S(1)} collective-permute-done((bf16[256,2048]{1,0:T(8,128)(2,1)S(1)}, bf16[256,2048]{1,0:T(8,128)(2,1)S(1)}, u32[]{:S(2)}, u32[]{:S(2)}) %collective-permute-start.2) | collective-permute-done | bytes 1048608 | tf_op jit(solution)/shard_map/ppermute | solution.py:144
  461.9 50.2 %collective-permute-done.3 = bf16[256,2048]{1,0:T(8,128)(2,1)S(1)} collective-permute-done((bf16[256,2048]{1,0:T(8,128)(2,1)S(1)}, bf16[256,2048]{1,0:T(8,128)(2,1)S(1)}, u32[]{:S(2)}, u32[]{:S(2)}) %collective-permute-start.3) | collective-permute-done | bytes 1048608 | tf_op jit(solution)/shard_map/ppermute | solution.py:144
  513.0 49.9 %collective-permute-done.4 = bf16[256,2048]{1,0:T(8,128)(2,1)S(1)} collective-permute-done((bf16[256,2048]{1,0:T(8,128)(2,1)S(1)}, bf16[256,2048]{1,0:T(8,128)(2,1)S(1)}, u32[]{:S(2)}, u32[]{:S(2)}) %collective-permute-start.4) | collective-permute-done | bytes 1048608 | tf_op jit(solution)/shard_map/ppermute | solution.py:144
  564.0 24.2 %collective-permute-done.5 = bf16[256,2048]{1,0:T(8,128)(2,1)} collective-permute-done((bf16[256,2048]{1,0:T(8,128)(2,1)S(1)}, bf16[256,2048]{1,0:T(8,128)(2,1)}, u32[]{:S(2)}, u32[]{:S(2)}) %collective-permute-start.5) | collective-permute-done | bytes 1048608 | tf_op jit(solution)/shard_map/ppermute | solution.py:144
  588.2 25.2 %collective-permute-done.6 = bf16[256,2048]{1,0:T(8,128)(2,1)} collective-permute-done((bf16[256,2048]{1,0:T(8,128)(2,1)}, bf16[256,2048]{1,0:T(8,128)(2,1)}, u32[]{:S(2)}, u32[]{:S(2)}) %collective-permute-start.6) | collective-permute-done | bytes 1048608 | tf_op jit(solution)/shard_map/ppermute | solution.py:144
  613.4 2.3 constant_dynamic-update-slice_fusion.15
  615.7 2.3 constant_dynamic-update-slice_fusion.14
  624.4 2.4 constant_dynamic-update-slice_fusion.7
  626.8 2.3 constant_dynamic-update-slice_fusion.6
  635.5 3.1 fusion.33
  638.6 25.9 %fusion.58 = bf16[1024,2048]{1,0:T(8,128)(2,1)} fusion(bf16[2048,2048]{1,0:T(8,128)(2,1)} %all-gather.20.cloned.1.call-done, bf16[4096,2048]{1,0:T(8,128)(2,1)} %constant_dynamic-update-slice_fusion, s32[]{:T(128)S(6)} %select_n.29, bf16[1024,2048]{1,0:T(8,128)(2,1)} %all-gather.18.cloned.1.call-done, f32[2048]{0:T(1024)S(1)} %copy-done.17, ...), kind=kOutput, calls=%fused_computation.67 | convolution fusion | flops 17196646400 | bytes 25178116 | tf_op jit(solution)/shard_map/dot_general | solution.py:63
  664.5 12.4 %reduce-scatter.5.cloned.1.call-done = bf16[1024,1024]{1,0:T(8,128)(2,1)} async-done(((bf16[1024,2048]{1,0:T(8,128)(2,1)}), bf16[1024,1024]{1,0:T(8,128)(2,1)}) %reduce-scatter.5.cloned.1.call-update) | async-done | bytes 2097168 | tf_op jit(solution)/shard_map/reduce_scatter | solution.py:152
  678.9 2.5 psum.15
  681.4 3.7 fusion.45
  (253 shorter events, 137.2 us)
Async XLA Ops:
  6.5 117.1 %copy-start = (bf16[2048,16]{0,1:T(8,128)(2,1)S(1)}, bf16[2048,16]{0,1:T(8,128)(2,1)}, u32[]{:S(2)}) copy-start(bf16[2048,16]{0,1:T(8,128)(2,1)} %param.23) | copy-start | bytes 196612
  6.5 22.0 %copy-start.12 = (f32[2048]{0:T(1024)S(1)}, f32[2048]{0:T(1024)}, u32[]{:S(2)}) copy-start(f32[2048]{0:T(1024)} %param.19) | copy-start | bytes 24580
  6.5 18.8 %all-gather.8.cloned.1.call-start = ((), (), s32[]{:S(2)}) async-start(), calls=%async_computation.2 | async-start | bytes 6291456 | tf_op jit(solution)/shard_map/all_gather | solution.py:85
  7.3 70.5 %all-gather.12.cloned.1.call-start = ((), (), s32[]{:S(2)}) async-start(), calls=%async_computation.4 | async-start | bytes 2359296 | tf_op jit(solution)/shard_map/all_gather | solution.py:97
  8.0 110.7 %all-gather.10.cloned.1.call-start = ((), (), s32[]{:S(2)}) async-start(), calls=%async_computation.3 | async-start | bytes 1179648 | tf_op jit(solution)/shard_map/all_gather | solution.py:95
  8.7 151.0 %all-gather.14.cloned.1.call-start = ((), (), s32[]{:S(2)}) async-start(), calls=%async_computation.5 | async-start | bytes 1179648 | tf_op jit(solution)/shard_map/all_gather | solution.py:94
  9.3 306.7 %all-gather.16.cloned.1.call-start = ((), (), s32[]{:S(2)}) async-start(), calls=%async_computation.6 | async-start | bytes 2359296 | tf_op jit(solution)/shard_map/all_gather | solution.py:131
  9.9 322.7 %reduce-scatter.3.cloned.1.call-start = ((), (), s32[]{:S(2)}) async-start(), calls=%async_computation.7 | async-start | bytes 6291456 | tf_op jit(solution)/shard_map/reduce_scatter | solution.py:132
  25.3 3.4 copy-start.3
  84.5 39.1 %copy-start.16 = (bf16[16,256]{1,0:T(8,128)(2,1)S(1)}, bf16[16,256]{1,0:T(8,128)(2,1)}, u32[]{:S(2)}) copy-start(bf16[16,256]{1,0:T(8,128)(2,1)} %param.24) | copy-start | bytes 24580
  84.5 39.1 %copy-start.18 = (f32[1024,1]{0,1:T(1,128)S(1)}, f32[1024,1]{0,1:T(1,128)}, u32[]{:S(2)}) copy-start(f32[1024,1]{0,1:T(1,128)} %param.26) | copy-start | bytes 12292
  84.5 39.1 %copy-start.19 = (f32[256]{0:T(256)S(1)}, f32[256]{0:T(256)}, u32[]{:S(2)}) copy-start(f32[256]{0:T(256)} %param.25) | copy-start | bytes 3076
  164.5 151.2 %copy-start.15 = (f32[512]{0:T(512)S(1)}, f32[512]{0:T(512)}, u32[]{:S(2)}) copy-start(f32[512]{0:T(512)} %param.27) | copy-start | bytes 6148
  321.9 15.3 %copy-start.4 = (bf16[1024,1024]{1,0:T(8,128)(2,1)S(1)}, bf16[1024,1024]{1,0:T(8,128)(2,1)}, u32[]{:S(2)}) copy-start(bf16[1024,1024]{1,0:T(8,128)(2,1)} %param.18) | copy-start | bytes 6291460
  321.9 15.3 %copy-start.13 = (f32[1024]{0:T(1024)S(1)}, f32[1024]{0:T(1024)}, u32[]{:S(2)}) copy-start(f32[1024]{0:T(1024)} %param.29) | copy-start | bytes 12292
  321.9 313.6 %all-gather.18.cloned.1.call-start = ((), (), s32[]{:S(2)}) async-start(), calls=%async_computation.8 | async-start | bytes 6291456 | tf_op jit(solution)/shard_map/all_gather | solution.py:140
  337.2 4.6 copy-start.5
  341.0 297.6 %all-gather.20.cloned.1.call-start = ((), (), s32[]{:S(2)}) async-start(), calls=%async_computation.9 | async-start | bytes 9437184 | tf_op jit(solution)/shard_map/all_gather | solution.py:151
  341.8 335.1 %reduce-scatter.5.cloned.1.call-start = ((), (), s32[]{:S(2)}) async-start(), calls=%async_computation.10 | async-start | bytes 6291456 | tf_op jit(solution)/shard_map/reduce_scatter | solution.py:152
  341.8 28.2 %collective-permute-start = (bf16[256,2048]{1,0:T(8,128)(2,1)S(1)}, bf16[256,2048]{1,0:T(8,128)(2,1)S(1)}, u32[]{:S(2)}, u32[]{:S(2)}) collective-permute-start(bf16[256,2048]{1,0:T(8,128)(2,1)S(1)} %copy-done.5), channel_id=1, source_target_pairs={{0,2},{2,4},{4,6},{6,8},{8,10},{10,12},{12,14},{14,0},{1,3},{3,5},... | collective-permute-start | bytes 3145736 | tf_op jit(solution)/shard_map/ppermute | solution.py:144
  370.0 48.4 %collective-permute-start.1 = (bf16[256,2048]{1,0:T(8,128)(2,1)S(1)}, bf16[256,2048]{1,0:T(8,128)(2,1)S(1)}, u32[]{:S(2)}, u32[]{:S(2)}) collective-permute-start(bf16[256,2048]{1,0:T(8,128)(2,1)S(1)} %collective-permute-done), channel_id=1, source_target_pairs={{0,2},{2,4},{4,6},{6,8},{8,10},{10,12},{12,14},{14,0},{1,3},{3,5},... | collective-permute-start | bytes 3145736 | tf_op jit(solution)/shard_map/ppermute | solution.py:144
  418.4 42.5 %collective-permute-start.2 = (bf16[256,2048]{1,0:T(8,128)(2,1)S(1)}, bf16[256,2048]{1,0:T(8,128)(2,1)S(1)}, u32[]{:S(2)}, u32[]{:S(2)}) collective-permute-start(bf16[256,2048]{1,0:T(8,128)(2,1)S(1)} %collective-permute-done.1), channel_id=1, source_target_pairs={{0,2},{2,4},{4,6},{6,8},{8,10},{10,12},{12,14},{14,0},{1,3},{3,5},... | collective-permute-start | bytes 3145736 | tf_op jit(solution)/shard_map/ppermute | solution.py:144
  460.9 1.0 copy-start.6
  461.9 50.2 %collective-permute-start.3 = (bf16[256,2048]{1,0:T(8,128)(2,1)S(1)}, bf16[256,2048]{1,0:T(8,128)(2,1)S(1)}, u32[]{:S(2)}, u32[]{:S(2)}) collective-permute-start(bf16[256,2048]{1,0:T(8,128)(2,1)S(1)} %collective-permute-done.2), channel_id=1, source_target_pairs={{0,2},{2,4},{4,6},{6,8},{8,10},{10,12},{12,14},{14,0},{1,3},{3,5},... | collective-permute-start | bytes 3145736 | tf_op jit(solution)/shard_map/ppermute | solution.py:144
  512.0 1.0 copy-start.8
  513.0 49.9 %collective-permute-start.4 = (bf16[256,2048]{1,0:T(8,128)(2,1)S(1)}, bf16[256,2048]{1,0:T(8,128)(2,1)S(1)}, u32[]{:S(2)}, u32[]{:S(2)}) collective-permute-start(bf16[256,2048]{1,0:T(8,128)(2,1)S(1)} %collective-permute-done.3), channel_id=1, source_target_pairs={{0,2},{2,4},{4,6},{6,8},{8,10},{10,12},{12,14},{14,0},{1,3},{3,5},... | collective-permute-start | bytes 3145736 | tf_op jit(solution)/shard_map/ppermute | solution.py:144
  563.0 1.0 copy-start.10
  564.0 24.2 %collective-permute-start.5 = (bf16[256,2048]{1,0:T(8,128)(2,1)S(1)}, bf16[256,2048]{1,0:T(8,128)(2,1)}, u32[]{:S(2)}, u32[]{:S(2)}) collective-permute-start(bf16[256,2048]{1,0:T(8,128)(2,1)S(1)} %collective-permute-done.4), channel_id=1, source_target_pairs={{0,2},{2,4},{4,6},{6,8},{8,10},{10,12},{12,14},{14,0},{1,3},{3,5},... | collective-permute-start | bytes 3145736 | tf_op jit(solution)/shard_map/ppermute | solution.py:144
  588.2 25.2 %collective-permute-start.6 = (bf16[256,2048]{1,0:T(8,128)(2,1)}, bf16[256,2048]{1,0:T(8,128)(2,1)}, u32[]{:S(2)}, u32[]{:S(2)}) collective-permute-start(bf16[256,2048]{1,0:T(8,128)(2,1)} %collective-permute-done.5), channel_id=1, source_target_pairs={{0,2},{2,4},{4,6},{6,8},{8,10},{10,12},{12,14},{14,0},{1,3},{3,5},... | collective-permute-start | bytes 3145736 | tf_op jit(solution)/shard_map/ppermute | solution.py:144
  588.2 29.9 %copy-start.11 = (bf16[256,2048]{1,0:T(8,128)(2,1)S(1)}, bf16[256,2048]{1,0:T(8,128)(2,1)}, u32[]{:S(2)}) copy-start(bf16[256,2048]{1,0:T(8,128)(2,1)} %copy-done.10) | copy-start | bytes 3145732
  588.2 30.9 %copy-start.9 = (bf16[256,2048]{1,0:T(8,128)(2,1)S(1)}, bf16[256,2048]{1,0:T(8,128)(2,1)}, u32[]{:S(2)}) copy-start(bf16[256,2048]{1,0:T(8,128)(2,1)} %copy-done.8) | copy-start | bytes 3145732
  588.2 31.9 %copy-start.7 = (bf16[256,2048]{1,0:T(8,128)(2,1)S(1)}, bf16[256,2048]{1,0:T(8,128)(2,1)}, u32[]{:S(2)}) copy-start(bf16[256,2048]{1,0:T(8,128)(2,1)} %copy-done.6) | copy-start | bytes 3145732
  633.4 5.2 copy-start.17
  664.5 17.0 %copy-start.2 = (bf16[1024,1024]{1,0:T(8,128)(2,1)S(1)}, bf16[1024,1024]{1,0:T(8,128)(2,1)}, u32[]{:S(2)}) copy-start(bf16[1024,1024]{1,0:T(8,128)(2,1)} %fusion.41) | copy-start | bytes 6291460
  664.5 17.0 %copy-start.14 = (f32[1024]{0:T(1024)S(1)}, f32[1024]{0:T(1024)}, u32[]{:S(2)}) copy-start(f32[1024]{0:T(1024)} %param.33) | copy-start | bytes 12292
  664.5 20.7 %copy-start.1 = (bf16[2048,16]{0,1:T(8,128)(2,1)S(1)}, bf16[2048,16]{0,1:T(8,128)(2,1)}, u32[]{:S(2)}) copy-start(bf16[2048,16]{0,1:T(8,128)(2,1)} %param.23) | copy-start | bytes 196612
Sparse Core Ops, SparseCore 0:
  8.9 16.3 all-gather.7
  27.4 50.2 all-gather.11
  79.8 38.7 all-gather.9
  120.7 38.9 all-gather.13
  161.6 49.1 all-gather.15
  322.0 10.5 reduce-scatter.2
  341.2 14.9 all-gather.17
  358.2 189.4 all-gather.19
  664.6 12.2 reduce-scatter.4
